TPU v7x, 32 devices: a whole 2x2x4 slice. The times are simulated.
32 devices in a mesh: ep: 8 (over z, core), tp: 4 (over y, x).
Axes of the slice: x: 2, y: 2, z: 4, core: 2. Of those that a mesh axis runs over, the one named last changes fastest.
Arguments:
- tokens: bfloat16 [512, 2048], P('ep', 'tp'), may hold values from -20 to 20
- state: float32 [512, 16, 64, 64], P('ep', 'tp'), may hold values from -1.5 to 1.5
- attn_gain: float32 [2048], replicated, may hold values from 0.1 to 1.9
- ffn_gain: float32 [2048], replicated, may hold values from 0.1 to 1.9
- w_query: bfloat16 [2048, 1024], P(None, 'tp'), may hold values from -0.125 to 0.125
- w_key: bfloat16 [2048, 1024], P(None, 'tp'), may hold values from -0.125 to 0.125
- w_value: bfloat16 [2048, 1024], P(None, 'tp'), may hold values from -0.125 to 0.125
- w_output_gate: bfloat16 [2048, 1024], P(None, 'tp'), may hold values from -0.125 to 0.125
- w_decay: bfloat16 [2048, 16], replicated, may hold values from -0.125 to 0.125
- w_beta: bfloat16 [2048, 16], replicated, may hold values from -0.125 to 0.125
- decay_rate: float32 [16], P('tp'), may hold values from 0.1 to 2
- decay_shift: float32 [16], P('tp'), may hold values from -2 to 1
- head_gain: float32 [64], replicated, may hold values from 0.1 to 1.9
- w_mix_out: bfloat16 [1024, 2048], P(None, 'tp'), may hold values from -0.1875 to 0.1875
- expert_ids: int32 [512, 2], P('ep'), may hold values from 0 to 7, all different within a row; in each aligned block of 64 rows (0 to 63, 64 to 127, ...) at most 32 rows name the same one
- expert_weights: float32 [512, 2], P('ep'), may hold values from 0.2 to 1
- w_gate: bfloat16 [8, 2048, 4096], P('ep', None, 'tp'), may hold values from -0.125 to 0.125
- w_up: bfloat16 [8, 2048, 4096], P('ep', None, 'tp'), may hold values from -0.125 to 0.125
- w_down: bfloat16 [8, 4096, 2048], P('ep', 'tp'), may hold values from -0.09375 to 0.09375
Outputs:
- layer_out: bfloat16 [512, 2048], P('ep', 'tp')
- new_state: float32 [512, 16, 64, 64], P('ep', 'tp')
Inputs may be any that keep to these rules, and one draw needn't show every extreme that they name: `expert_ids`: each row names 2 different experts; within the rows of one index of ep (aligned blocks of 64 rows) no expert is named by more than 32 rows, and in some blocks one expert is named by exactly 32 rows.
All inputs are finite; a program needn't handle non-finite values.
Results may differ from a plain program's by a relative error of at most 0.013.
Values may be sent and summed in bfloat16 or wider, within the bound.
A program may use at most 64 MiB of HBM per device.

v0:
```python
import jax
import jax.numpy as jnp
from jax import lax
from jax.sharding import PartitionSpec as P

EPS = 1e-06


def unit_norm(values):
    return values * lax.rsqrt(jnp.sum(values * values, axis=-1, keepdims=True) + EPS)


def stored(values):
    return lax.optimization_barrier(values.astype(jnp.bfloat16)).astype(jnp.float32)


def shards(
    tokens,
    state,
    attn_gain,
    ffn_gain,
    w_query,
    w_key,
    w_value,
    w_output_gate,
    w_decay,
    w_beta,
    decay_rate,
    decay_shift,
    head_gain,
    w_mix_out,
    expert_ids,
    expert_weights,
    w_gate,
    w_up,
    w_down,
):
    groups = lax.axis_size("ep")
    seq_count = tokens.shape[0]
    own_width = tokens.shape[1]
    model_width = ffn_gain.shape[0]
    head_dim = head_gain.shape[0]
    heads_here = decay_rate.shape[0]
    top_count = expert_ids.shape[1]
    local_experts = w_gate.shape[0]
    expert_total = local_experts * groups
    capacity = max(2, 2 * seq_count * top_count // expert_total)
    whole_rows = lax.all_gather(tokens, "tp", axis=1, tiled=True)
    whole_f32 = whole_rows.astype(jnp.float32)
    normed = (
        whole_f32
        * lax.rsqrt(jnp.mean(whole_f32 * whole_f32, axis=1, keepdims=True) + EPS)
        * attn_gain
    ).astype(jnp.bfloat16)

    def project(weight):
        return jnp.dot(normed, weight, preferred_element_type=jnp.float32)

    def by_head(values):
        return values.reshape(seq_count, heads_here, head_dim)

    first_head = lax.axis_index("tp") * heads_here
    decay_cols = lax.dynamic_slice_in_dim(w_decay, first_head, heads_here, 1)
    beta_cols = lax.dynamic_slice_in_dim(w_beta, first_head, heads_here, 1)
    query_proj = stored(project(w_query))
    key_proj = stored(project(w_key))
    value_proj = stored(project(w_value))
    gate_proj = stored(project(w_output_gate))
    keep_rate = jnp.exp(-decay_rate * jax.nn.softplus(project(decay_cols) + decay_shift))
    beta_gate = jax.nn.sigmoid(project(beta_cols))
    query_head = unit_norm(jax.nn.silu(by_head(query_proj))) * head_dim ** (-0.5)
    key_head = unit_norm(jax.nn.silu(by_head(key_proj)))
    value_head = jax.nn.silu(by_head(value_proj))
    decayed = keep_rate[:, :, None, None] * state
    recalled = jnp.einsum("thd,thde->the", key_head, decayed, precision=lax.Precision.HIGHEST)
    correction = beta_gate[:, :, None] * (value_head - recalled)
    new_state = decayed + key_head[:, :, :, None] * correction[:, :, None, :]
    reading = jnp.einsum("thd,thde->the", query_head, new_state, precision=lax.Precision.HIGHEST)
    reading_scale = lax.rsqrt(jnp.mean(reading * reading, axis=-1, keepdims=True) + EPS)
    head_out = (reading * reading_scale * head_gain * jax.nn.silu(by_head(gate_proj))).astype(
        jnp.bfloat16
    )
    head_out = head_out.reshape(seq_count, heads_here * head_dim)
    mixed = jnp.dot(
        lax.all_gather(head_out, "tp", axis=1, tiled=True),
        w_mix_out,
        preferred_element_type=jnp.float32,
    )
    residual = (tokens.astype(jnp.float32) + mixed).astype(jnp.bfloat16)
    residual_f32 = residual.astype(jnp.float32)
    pair_count = seq_count * top_count
    flat_ids = expert_ids.reshape(pair_count)
    one_hot = (flat_ids[:, None] == jnp.arange(expert_total, dtype=jnp.int32)[None, :]).astype(
        jnp.int32
    )
    pair_index = jnp.arange(pair_count, dtype=jnp.int32)
    lower_mask = (pair_index[:, None] > pair_index[None, :]).astype(jnp.int32)
    earlier = jnp.dot(lower_mask, one_hot)
    slot_rank = jnp.sum(earlier * one_hot, axis=1)
    slot_of = flat_ids * capacity + slot_rank
    slot_count = expert_total * capacity
    slot_hit = jnp.arange(slot_count, dtype=jnp.int32)[:, None] == slot_of[None, :]
    dispatch = slot_hit.astype(jnp.bfloat16)
    dispatch_tokens = jnp.any(slot_hit.reshape(slot_count, seq_count, top_count), axis=2).astype(
        jnp.bfloat16
    )
    own_gain = lax.dynamic_slice_in_dim(ffn_gain, lax.axis_index("tp") * own_width, own_width, 0)
    square_total = lax.psum(jnp.sum(residual_f32 * residual_f32, axis=1), "tp")
    row_scale = lax.rsqrt(square_total / model_width + EPS)
    normed_ffn = (residual_f32 * row_scale[:, None] * own_gain).astype(jnp.bfloat16)
    outgoing = jnp.dot(dispatch_tokens, normed_ffn, preferred_element_type=jnp.float32).astype(
        jnp.bfloat16
    )
    arrived = lax.all_to_all(outgoing, "ep", split_axis=0, concat_axis=0, tiled=True)
    segment = lax.all_gather(arrived, "tp", axis=1, tiled=True)
    blocks = segment.reshape(groups, local_experts, capacity, segment.shape[1])
    gate_part = jnp.einsum("secd,edf->secf", blocks, w_gate, preferred_element_type=jnp.float32)
    up_part = jnp.einsum("secd,edf->secf", blocks, w_up, preferred_element_type=jnp.float32)
    expert_hidden = (jax.nn.silu(gate_part) * up_part).astype(jnp.bfloat16)
    partial_value = jnp.einsum(
        "secf,efd->secd", expert_hidden, w_down, preferred_element_type=jnp.float32
    )
    partial_value = partial_value.astype(jnp.bfloat16).reshape(
        groups * local_experts * capacity, model_width
    )
    summed = lax.psum_scatter(
        partial_value.astype(jnp.float32).astype(jnp.bfloat16),
        "tp",
        scatter_dimension=1,
        tiled=True,
    )
    returned = lax.all_to_all(summed, "ep", split_axis=0, concat_axis=0, tiled=True)
    pair_rows = jnp.einsum("sp,sd->pd", dispatch, returned, preferred_element_type=jnp.float32)
    weighted = jnp.sum(
        pair_rows.reshape(seq_count, top_count, own_width) * expert_weights[:, :, None], axis=1
    )
    layer_out = (residual_f32 + weighted).astype(jnp.bfloat16)
    return (layer_out, new_state)


def solution(mesh):
    in_specs = (
        P("ep", "tp"),
        P("ep", "tp", None, None),
        P(),
        P(),
        P(None, "tp"),
        P(None, "tp"),
        P(None, "tp"),
        P(None, "tp"),
        P(),
        P(),
        P("tp"),
        P("tp"),
        P(),
        P(None, "tp"),
        P("ep", None),
        P("ep", None),
        P("ep", None, "tp"),
        P("ep", None, "tp"),
        P("ep", "tp", None),
    )
    out_specs = (P("ep", "tp"), P("ep", "tp", None, None))
    return jax.shard_map(shards, mesh=mesh, in_specs=in_specs, out_specs=out_specs, check_vma=False)
```

profile of v0, /device:TPU:0, one launch (start us, length us, event | category | flops | bytes accessed | tf_op | source)
XLA Modules:
  0.0 171.2 jit_solution(3074201662367445162)
XLA Ops:
  7.2 10.9 %all_gather.9 = bf16[64,2048]{1,0:T(8,128)(2,1)S(1)} all-gather(bf16[64,512]{1,0:T(8,128)(2,1)} %param.19), channel_id=1, replica_groups=mesh['ep'=8,'tp'=4] {'tp'}, dimensions={1}, use_global_device_ids=true | all-gather | bytes 327680 | tf_op jit(solution)/shard_map/all_gather | solution.py:48
  18.1 0.2 fusion.36
  18.3 1.6 convolution_convert_fusion.3
  19.9 0.1 reshape.179
  20.0 0.2 multiply_reduce_fusion.2
  20.2 0.1 broadcast_multiply_fusion
  20.3 0.7 neg.32
  21.0 1.0 fusion.51
  22.0 0.1 copy.39
  22.1 1.0 fusion.33
  23.2 0.1 copy.40
  23.3 1.6 convolution_convert_fusion.2
  24.9 0.1 reshape.181
  25.0 10.1 %fusion = f32[64,4,1,64]{3,2,1,0:T(1,128)S(1)} fusion(f32[64,4,64,1]{2,3,1,0:T(1,128)S(1)} %bitcast.87, f32[64,4,64,64]{3,2,1,0:T(8,128)} %param.20, f32[64,4]{1,0:T(8,128)S(1)} %copy.39), kind=kOutput, calls=%fused_computation.1 | convolution fusion | flops 13631488 | bytes 4326400 | tf_op jit(solution)/shard_map/thd,thde->the/dot_general | solution.py:75
  35.1 0.1 fusion.42
  35.3 5.2 %multiply_add_fusion = f32[64,4,64,64]{3,2,1,0:T(8,128)} fusion(f32[64,4,64,64]{3,2,1,0:T(8,128)S(1)} %copy-done.1, f32[64,4,64]{2,1,0:T(4,128)S(1)} %fusion.42, f32[64,4,64]{2,1,0:T(4,128)S(1)} %broadcast_multiply_fusion, f32[64,4]{1,0:T(8,128)S(1)} %copy.39), kind=kLoop, calls=%fused_computation | loop fusion | flops 3145728 | bytes 8520704 | tf_op jit(solution)/shard_map/add | solution.py:77
  40.6 0.3 convolution_convert_fusion.4
  40.9 0.1 reshape.177
  41.0 0.2 multiply_reduce_fusion.3
  41.2 0.1 multiply_multiply_fusion
  41.4 9.5 %fusion.64 = f32[64,4,1,64]{3,2,1,0:T(1,128)S(1)} fusion(f32[64,4,64,1]{2,3,1,0:T(1,128)S(1)} %bitcast.95, f32[64,4,64,64]{3,2,1,0:T(8,128)} %multiply_add_fusion), kind=kOutput, calls=%fused_computation.79 | convolution fusion | flops 12582912 | bytes 4325376 | tf_op jit(solution)/shard_map/thd,thde->the/dot_general | solution.py:78
  50.9 0.1 multiply_reduce_fusion.1
  51.0 0.3 convolution_convert_fusion.1
  51.4 0.1 reshape.183
  51.5 0.1 fusion.44
  51.7 0.1 reshape.168
  51.8 8.7 %all_gather.10 = bf16[64,1024]{1,0:T(8,128)(2,1)S(1)} all-gather(bf16[64,256]{1,0:T(8,128)(2,1)S(1)} %reshape.168), channel_id=1, replica_groups=mesh['ep'=8,'tp'=4] {'tp'}, dimensions={1}, use_global_device_ids=true | all-gather | bytes 163840 | tf_op jit(solution)/shard_map/all_gather | solution.py:85
  60.5 0.4 multiply_reduce_fusion
  60.9 8.9 %psum.7 = f32[64]{0:T(128)S(1)} all-reduce(f32[64]{0:T(128)S(1)} %get-tuple-element.2), channel_id=1, replica_groups=mesh['ep'=8,'tp'=4] {'tp'}, use_global_device_ids=true, to_apply=%region_7.8 | all-reduce | flops 64 | bytes 512 | tf_op jit(solution)/shard_map/psum | solution.py:108
  69.8 0.1 copy.41
  69.9 0.1 reshape.169
  70.0 0.1 fusion.30
  70.2 0.2 reduce_sum.70
  70.4 0.1 copy.42
  70.4 0.1 fusion.43
  70.6 0.8 dynamic_slice.11
  71.3 0.3 convolution_convert_fusion
  71.6 14.5 %all_to_all.24 = bf16[8,32,512]{2,1,0:T(8,128)(2,1)} all-to-all(bf16[8,32,512]{2,1,0:T(8,128)(2,1)S(1)} %bitcast.90), channel_id=1, replica_groups=mesh['ep'=8,'tp'=4] {'ep'}, dimensions={0} | all-to-all | bytes 524288 | tf_op jit(solution)/shard_map/all_to_all | solution.py:114
  86.1 0.0 reduce-scatter.2.cloned.1.call-start
  86.2 23.8 %all-gather.2.cloned.1.call-done = bf16[256,2048]{1,0:T(8,128)(2,1)} async-done(((bf16[256,512]{1,0:T(8,128)(2,1)}), bf16[256,2048]{1,0:T(8,128)(2,1)}) %all-gather.2.cloned.1.call-update) | async-done | bytes 1048592 | tf_op jit(solution)/shard_map/all_gather | solution.py:115
  110.0 3.8 %fusion.12 = f32[8,1,32,1024]{3,2,0,1:T(8,128)S(1)} fusion(bf16[8,32,2048]{2,1,0:T(8,128)(2,1)} %bitcast.97, bf16[1,2048,1024]{2,1,0:T(8,128)(2,1)} %param.35), kind=kOutput, calls=%fused_computation.11 | convolution fusion | flops 1073741824 | bytes 6291456 | tf_op jit(solution)/shard_map/secd,edf->secf/dot_general | solution.py:117
  113.7 7.4 %fusion.9 = bf16[8,32,2048]{2,1,0:T(8,128)(2,1)} fusion(bf16[1,1024,2048]{2,1,0:T(8,128)(2,1)} %param.37, bf16[8,32,2048]{2,1,0:T(8,128)(2,1)} %bitcast.98, bf16[1,2048,1024]{2,1,0:T(8,128)(2,1)} %param.36, f32[8,1,32,1024]{3,2,0,1:T(8,128)S(1)} %fusion.12), kind=kOutput, calls=%fused_computation.10 | convolution fusion | flops 2149580800 | bytes 11534336 | tf_op jit(solution)/shard_map/secf,efd->secd/dot_general | solution.py:120
  121.1 28.1 %reduce-scatter.2.cloned.1.call-done = bf16[256,512]{1,0:T(8,128)(2,1)} async-done(((bf16[256,2048]{1,0:T(8,128)(2,1)}), bf16[256,512]{1,0:T(8,128)(2,1)}) %reduce-scatter.2.cloned.1.call-update) | async-done | bytes 262160 | tf_op jit(solution)/shard_map/reduce_scatter | solution.py:126
  149.2 4.6 %all-to-all-start.1 = ((bf16[8,32,512]{2,1,0:T(8,128)(2,1)}), bf16[8,32,512]{2,1,0:T(8,128)(2,1)S(1)}, u32[]{:S(2)}, u32[]{:S(2)}) async-start(bf16[8,32,512]{2,1,0:T(8,128)(2,1)} %bitcast.96), calls=%async_computation.2 | async-start | bytes 524288 | tf_op jit(solution)/shard_map/all_to_all | solution.py:132
  153.8 0.1 iota_compare_fusion.1
  154.0 9.6 %all-to-all-done.1 = bf16[8,32,512]{2,1,0:T(8,128)(2,1)S(1)} async-done(((bf16[8,32,512]{2,1,0:T(8,128)(2,1)}), bf16[8,32,512]{2,1,0:T(8,128)(2,1)S(1)}, u32[]{:S(2)}, u32[]{:S(2)}) %all-to-all-start.1) | async-done | bytes 262176 | tf_op jit(solution)/shard_map/all_to_all | solution.py:132
  163.5 0.2 fusion.27
  163.7 0.7 add_convert_fusion
  (29 shorter events, 0.2 us)
Async XLA Ops:
  7.2 53.3 %copy-start = (bf16[1024,512]{1,0:T(8,128)(2,1)S(1)}, bf16[1024,512]{1,0:T(8,128)(2,1)}, u32[]{:S(2)}) copy-start(bf16[1024,512]{1,0:T(8,128)(2,1)} %param.32) | copy-start | bytes 3145732
  7.2 102.8 %all-gather.2.cloned.1.call-start = ((), (), s32[]{:S(2)}) async-start(), calls=%async_computation.3 | async-start | bytes 1310720 | tf_op jit(solution)/shard_map/all_gather | solution.py:115
  25.0 10.3 %copy-start.1 = (f32[64,4,64,64]{3,2,1,0:T(8,128)S(1)}, f32[64,4,64,64]{3,2,1,0:T(8,128)}, u32[]{:S(2)}) copy-start(f32[64,4,64,64]{3,2,1,0:T(8,128)} %param.20) | copy-start | bytes 12582916
  35.3 5.2 %copy-start.2 = (bf16[2048,256]{1,0:T(8,128)(2,1)S(1)}, bf16[2048,256]{1,0:T(8,128)(2,1)}, u32[]{:S(2)}) copy-start(bf16[2048,256]{1,0:T(8,128)(2,1)} %param.23) | copy-start | bytes 3145732
  35.3 5.2 %copy-start.5 = (f32[2048]{0:T(1024)S(1)}, f32[2048]{0:T(1024)}, u32[]{:S(2)}) copy-start(f32[2048]{0:T(1024)} %param.21) | copy-start | bytes 24580
  40.5 10.5 %copy-start.3 = (bf16[2048,256]{1,0:T(8,128)(2,1)S(1)}, bf16[2048,256]{1,0:T(8,128)(2,1)}, u32[]{:S(2)}) copy-start(bf16[2048,256]{1,0:T(8,128)(2,1)} %param.26) | copy-start | bytes 3145732
  40.5 11.0 %copy-start.8 = (f32[64]{0:T(128)S(1)}, f32[64]{0:T(128)}, u32[]{:S(2)}) copy-start(f32[64]{0:T(128)} %param.31) | copy-start | bytes 772
  40.5 19.9 %copy-start.4 = (bf16[64,512]{1,0:T(8,128)(2,1)S(1)}, bf16[64,512]{1,0:T(8,128)(2,1)}, u32[]{:S(2)}) copy-start(bf16[64,512]{1,0:T(8,128)(2,1)} %param.19) | copy-start | bytes 196612
  40.5 29.3 %copy-start.6 = (s32[64,2]{0,1:T(2,128)S(1)}, s32[64,2]{0,1:T(2,128)}, u32[]{:S(2)}) copy-start(s32[64,2]{0,1:T(2,128)} %param.33) | copy-start | bytes 1540
  86.1 63.1 %reduce-scatter.2.cloned.1.call-start = ((), (), s32[]{:S(2)}) async-start(), calls=%async_computation.4 | async-start | bytes 1310720 | tf_op jit(solution)/shard_map/reduce_scatter | solution.py:126
  113.7 49.8 %copy-start.7 = (f32[64,2]{0,1:T(2,128)S(1)}, f32[64,2]{0,1:T(2,128)}, u32[]{:S(2)}) copy-start(f32[64,2]{0,1:T(2,128)} %param.34) | copy-start | bytes 1540
  149.2 14.3 %all-to-all-start.1 = ((bf16[8,32,512]{2,1,0:T(8,128)(2,1)}), bf16[8,32,512]{2,1,0:T(8,128)(2,1)S(1)}, u32[]{:S(2)}, u32[]{:S(2)}) async-start(bf16[8,32,512]{2,1,0:T(8,128)(2,1)} %bitcast.96), calls=%async_computation.2 | async-start | bytes 524288 | tf_op jit(solution)/shard_map/all_to_all | solution.py:132
Sparse Core Ops, SparseCore 0:
  86.2 23.6 all-gather.1
  121.2 27.9 reduce-scatter.1
where the time goes:
time: 172 us; the launch traced here: 171 us
  waiting for transfers between devices  61.5 us (36%)
  blocking collectives  43 us (25%)
  matrix products  37.7 us (22%)
  between operations  14.3 us (8%)
  other arithmetic  7.97 us (5%)
  starting transfers between devices  4.68 us (3%)
  local copies, waits for them, and re-layouts  2.11 us (1%)
    reduce_scatter x1, waiting for transfers between devices, shards(): lax.psum_scatter(partial_value.astype(jnp.float32).astype(jnp.bfloat16),...  28.1 us
    all_gather x1, waiting for transfers between devices, shards(): segment = lax.all_gather(arrived, 'tp', axis=1, tiled=True)  23.8 us
    all_to_all x1, blocking collectives, shards(): lax.all_to_all(outgoing, 'ep', split_axis=0, concat_axis=0, tiled=True)  14.5 us
    all_gather x1, blocking collectives, shards(): whole_rows = lax.all_gather(tokens, 'tp', axis=1, tiled=True)  10.9 us
    dot_general x1, matrix products, shards(): jnp.einsum('thd,thde->the', key_head, decayed, precision=lax.Precision.HI...  10.1 us
    all_to_all x1, waiting for transfers between devices, shards(): lax.all_to_all(summed, 'ep', split_axis=0, concat_axis=0, tiled=True)  9.56 us
    dot_general x1, matrix products, shards(): jnp.einsum('thd,thde->the', query_head, new_state, precision=lax.Precisio...  9.48 us
    psum x1, blocking collectives, shards(): square_total = lax.psum(jnp.sum(residual_f32 * residual_f32, axis=1), 'tp')  8.93 us
  transfers between devices with their start and end apart: 3, of which 3 were waited for; matrix products, arithmetic and copies ran while one was open for 0% of the time, Pallas kernels for 0%

commit v1 on v0

--- a/solution.py
+++ b/solution.py
@@ -105,7 +105,9 @@
         jnp.bfloat16
     )
     own_gain = lax.dynamic_slice_in_dim(ffn_gain, lax.axis_index("tp") * own_width, own_width, 0)
-    square_total = lax.psum(jnp.sum(residual_f32 * residual_f32, axis=1), "tp")
+    square_total = jnp.sum(
+        lax.all_gather(jnp.sum(residual_f32 * residual_f32, axis=1), "tp"), axis=0
+    )
     row_scale = lax.rsqrt(square_total / model_width + EPS)
     normed_ffn = (residual_f32 * row_scale[:, None] * own_gain).astype(jnp.bfloat16)
     outgoing = jnp.dot(dispatch_tokens, normed_ffn, preferred_element_type=jnp.float32).astype(

time: 172 us -> 174 us (1.012)
    unnamed x0 -> x1, blocking collectives: none -> 9.07 us
    psum x1 -> x0, blocking collectives: 8.93 us -> none  [shards(): square_total = lax.psum(jnp.sum(residual_f32 * residual_f32, axis=1), 'tp')]
where the time goes in v1:
time: 174 us; the launch traced here: 173 us
  waiting for transfers between devices  61.5 us (35%)
  blocking collectives  43.1 us (25%)
  matrix products  37.6 us (22%)
  between operations  15 us (9%)
  other arithmetic  8.03 us (5%)
  starting transfers between devices  4.68 us (3%)
  local copies, waits for them, and re-layouts  3.03 us (2%)
    reduce_scatter x1, waiting for transfers between devices, shards(): lax.psum_scatter(partial_value.astype(jnp.float32).astype(jnp.bfloat16),...  28.1 us
    all_gather x1, waiting for transfers between devices, shards(): segment = lax.all_gather(arrived, 'tp', axis=1, tiled=True)  23.8 us
    all_to_all x1, blocking collectives, shards(): lax.all_to_all(outgoing, 'ep', split_axis=0, concat_axis=0, tiled=True)  14.5 us
    all_gather x1, blocking collectives, shards(): whole_rows = lax.all_gather(tokens, 'tp', axis=1, tiled=True)  10.9 us
    dot_general x1, matrix products, shards(): jnp.einsum('thd,thde->the', key_head, decayed, precision=lax.Precision.HI...  10.1 us
    all_to_all x1, waiting for transfers between devices, shards(): lax.all_to_all(summed, 'ep', split_axis=0, concat_axis=0, tiled=True)  9.56 us
    dot_general x1, matrix products, shards(): jnp.einsum('thd,thde->the', query_head, new_state, precision=lax.Precisio...  9.48 us
    unnamed x1, blocking collectives  9.07 us
  transfers between devices with their start and end apart: 3, of which 3 were waited for; matrix products, arithmetic and copies ran while one was open for 0% of the time, Pallas kernels for 0%

profile of v1, /device:TPU:0, one launch (start us, length us, event | category | flops | bytes accessed | tf_op | source)
XLA Modules:
  0.0 173.0 jit_solution(3734806167504415430)
XLA Ops:
  7.2 10.9 %all_gather.15 = bf16[64,2048]{1,0:T(8,128)(2,1)S(1)} all-gather(bf16[64,512]{1,0:T(8,128)(2,1)} %param.19), channel_id=1, replica_groups=mesh['ep'=8,'tp'=4] {'tp'}, dimensions={1}, use_global_device_ids=true | all-gather | bytes 327680 | tf_op jit(solution)/shard_map/all_gather | solution.py:48
  18.1 0.2 fusion.36
  18.3 1.6 convolution_convert_fusion.3
  19.9 0.1 reshape.183
  20.0 0.2 multiply_reduce_fusion.2
  20.2 0.1 broadcast_multiply_fusion
  20.3 0.7 neg.32
  21.0 1.0 fusion.51
  22.0 0.1 copy.39
  22.1 1.0 fusion.33
  23.2 0.1 copy.40
  23.3 1.6 convolution_convert_fusion.2
  24.9 0.1 reshape.185
  25.0 10.1 %fusion = f32[64,4,1,64]{3,2,1,0:T(1,128)S(1)} fusion(f32[64,4,64,1]{2,3,1,0:T(1,128)S(1)} %bitcast.88, f32[64,4,64,64]{3,2,1,0:T(8,128)} %param.20, f32[64,4]{1,0:T(8,128)S(1)} %copy.39), kind=kOutput, calls=%fused_computation.1 | convolution fusion | flops 13631488 | bytes 4326400 | tf_op jit(solution)/shard_map/thd,thde->the/dot_general | solution.py:75
  35.1 0.1 fusion.42
  35.3 5.2 %multiply_add_fusion = f32[64,4,64,64]{3,2,1,0:T(8,128)} fusion(f32[64,4,64,64]{3,2,1,0:T(8,128)S(1)} %copy-done.1, f32[64,4,64]{2,1,0:T(4,128)S(1)} %fusion.42, f32[64,4,64]{2,1,0:T(4,128)S(1)} %broadcast_multiply_fusion, f32[64,4]{1,0:T(8,128)S(1)} %copy.39), kind=kLoop, calls=%fused_computation | loop fusion | flops 3145728 | bytes 8520704 | tf_op jit(solution)/shard_map/add | solution.py:77
  40.6 0.3 convolution_convert_fusion.4
  41.0 0.1 reshape.181
  41.1 0.2 multiply_reduce_fusion.3
  41.3 0.1 multiply_multiply_fusion
  41.4 9.5 %fusion.64 = f32[64,4,1,64]{3,2,1,0:T(1,128)S(1)} fusion(f32[64,4,64,1]{2,3,1,0:T(1,128)S(1)} %bitcast.96, f32[64,4,64,64]{3,2,1,0:T(8,128)} %multiply_add_fusion), kind=kOutput, calls=%fused_computation.79 | convolution fusion | flops 12582912 | bytes 4325376 | tf_op jit(solution)/shard_map/thd,thde->the/dot_general | solution.py:78
  50.9 0.1 multiply_reduce_fusion.1
  51.1 0.3 convolution_convert_fusion.1
  51.4 0.1 reshape.187
  51.6 0.1 fusion.44
  51.7 0.1 reshape.172
  51.8 8.7 %all_gather.16 = bf16[64,1024]{1,0:T(8,128)(2,1)S(1)} all-gather(bf16[64,256]{1,0:T(8,128)(2,1)S(1)} %reshape.172), channel_id=1, replica_groups=mesh['ep'=8,'tp'=4] {'tp'}, dimensions={1}, use_global_device_ids=true | all-gather | bytes 163840 | tf_op jit(solution)/shard_map/all_gather | solution.py:85
  60.5 0.4 multiply_reduce_fusion
  60.9 0.6 dynamic-slice
  62.2 0.2 dynamic-update-slice
  62.4 9.1 %all-reduce = f32[256]{0:T(256)S(1)} all-reduce(f32[256]{0:T(256)S(1)} %dynamic-update-slice), channel_id=2, replica_groups=mesh['ep'=8,'tp'=4] {'tp'}, use_global_device_ids=true, to_apply=%add | all-reduce | flops 256 | bytes 2048
  71.6 0.1 copy.41
  71.7 0.1 reshape.173
  71.8 0.1 fusion.30
  72.0 0.2 reduce_sum.79
  72.2 0.1 fusion.43
  72.3 0.8 dynamic_slice.11
  73.1 0.3 convolution_convert_fusion
  73.4 14.5 %all_to_all.24 = bf16[8,32,512]{2,1,0:T(8,128)(2,1)} all-to-all(bf16[8,32,512]{2,1,0:T(8,128)(2,1)S(1)} %bitcast.91), channel_id=1, replica_groups=mesh['ep'=8,'tp'=4] {'ep'}, dimensions={0} | all-to-all | bytes 524288 | tf_op jit(solution)/shard_map/all_to_all | solution.py:116
  88.0 23.8 %all-gather.3.cloned.1.call-done = bf16[256,2048]{1,0:T(8,128)(2,1)} async-done(((bf16[256,512]{1,0:T(8,128)(2,1)}), bf16[256,2048]{1,0:T(8,128)(2,1)}) %all-gather.3.cloned.1.call-update) | async-done | bytes 1048592 | tf_op jit(solution)/shard_map/all_gather | solution.py:117
  111.8 3.8 %fusion.12 = f32[8,1,32,1024]{3,2,0,1:T(8,128)S(1)} fusion(bf16[8,32,2048]{2,1,0:T(8,128)(2,1)} %bitcast.98, bf16[1,2048,1024]{2,1,0:T(8,128)(2,1)} %param.35), kind=kOutput, calls=%fused_computation.11 | convolution fusion | flops 1073741824 | bytes 6291456 | tf_op jit(solution)/shard_map/secd,edf->secf/dot_general | solution.py:119
  115.5 7.4 %fusion.9 = bf16[8,32,2048]{2,1,0:T(8,128)(2,1)} fusion(bf16[1,1024,2048]{2,1,0:T(8,128)(2,1)} %param.37, bf16[8,32,2048]{2,1,0:T(8,128)(2,1)} %bitcast.99, bf16[1,2048,1024]{2,1,0:T(8,128)(2,1)} %param.36, f32[8,1,32,1024]{3,2,0,1:T(8,128)S(1)} %fusion.12), kind=kOutput, calls=%fused_computation.10 | convolution fusion | flops 2149580800 | bytes 11534336 | tf_op jit(solution)/shard_map/secf,efd->secd/dot_general | solution.py:122
  122.9 28.1 %reduce-scatter.2.cloned.1.call-done = bf16[256,512]{1,0:T(8,128)(2,1)} async-done(((bf16[256,2048]{1,0:T(8,128)(2,1)}), bf16[256,512]{1,0:T(8,128)(2,1)}) %reduce-scatter.2.cloned.1.call-update) | async-done | bytes 262160 | tf_op jit(solution)/shard_map/reduce_scatter | solution.py:128
  151.0 4.6 %all-to-all-start.1 = ((bf16[8,32,512]{2,1,0:T(8,128)(2,1)}), bf16[8,32,512]{2,1,0:T(8,128)(2,1)S(1)}, u32[]{:S(2)}, u32[]{:S(2)}) async-start(bf16[8,32,512]{2,1,0:T(8,128)(2,1)} %bitcast.97), calls=%async_computation.2 | async-start | bytes 524288 | tf_op jit(solution)/shard_map/all_to_all | solution.py:134
  155.6 0.1 iota_compare_fusion.1
  155.8 9.6 %all-to-all-done.1 = bf16[8,32,512]{2,1,0:T(8,128)(2,1)S(1)} async-done(((bf16[8,32,512]{2,1,0:T(8,128)(2,1)}), bf16[8,32,512]{2,1,0:T(8,128)(2,1)S(1)}, u32[]{:S(2)}, u32[]{:S(2)}) %all-to-all-start.1) | async-done | bytes 262176 | tf_op jit(solution)/shard_map/all_to_all | solution.py:134
  165.3 0.2 fusion.27
  165.5 0.7 add_convert_fusion
  (36 shorter events, 0.5 us)
Async XLA Ops:
  7.2 53.4 %copy-start = (bf16[1024,512]{1,0:T(8,128)(2,1)S(1)}, bf16[1024,512]{1,0:T(8,128)(2,1)}, u32[]{:S(2)}) copy-start(bf16[1024,512]{1,0:T(8,128)(2,1)} %param.32) | copy-start | bytes 3145732
  7.2 104.6 %all-gather.3.cloned.1.call-start = ((), (), s32[]{:S(2)}) async-start(), calls=%async_computation.3 | async-start | bytes 1310720 | tf_op jit(solution)/shard_map/all_gather | solution.py:117
  25.0 10.3 %copy-start.1 = (f32[64,4,64,64]{3,2,1,0:T(8,128)S(1)}, f32[64,4,64,64]{3,2,1,0:T(8,128)}, u32[]{:S(2)}) copy-start(f32[64,4,64,64]{3,2,1,0:T(8,128)} %param.20) | copy-start | bytes 12582916
  35.3 5.3 %copy-start.2 = (bf16[2048,256]{1,0:T(8,128)(2,1)S(1)}, bf16[2048,256]{1,0:T(8,128)(2,1)}, u32[]{:S(2)}) copy-start(bf16[2048,256]{1,0:T(8,128)(2,1)} %param.23) | copy-start | bytes 3145732
  35.3 5.3 %copy-start.5 = (f32[2048]{0:T(1024)S(1)}, f32[2048]{0:T(1024)}, u32[]{:S(2)}) copy-start(f32[2048]{0:T(1024)} %param.21) | copy-start | bytes 24580
  40.6 10.5 %copy-start.3 = (bf16[2048,256]{1,0:T(8,128)(2,1)S(1)}, bf16[2048,256]{1,0:T(8,128)(2,1)}, u32[]{:S(2)}) copy-start(bf16[2048,256]{1,0:T(8,128)(2,1)} %param.26) | copy-start | bytes 3145732
  40.6 11.0 %copy-start.8 = (f32[64]{0:T(128)S(1)}, f32[64]{0:T(128)}, u32[]{:S(2)}) copy-start(f32[64]{0:T(128)} %param.31) | copy-start | bytes 772
  40.6 19.9 %copy-start.4 = (bf16[64,512]{1,0:T(8,128)(2,1)S(1)}, bf16[64,512]{1,0:T(8,128)(2,1)}, u32[]{:S(2)}) copy-start(bf16[64,512]{1,0:T(8,128)(2,1)} %param.19) | copy-start | bytes 196612
  40.6 20.3 %copy-start.9 = (u32[32]{0:T(128)S(1)}, u32[32]{0:T(128)}, u32[]{:S(2)}) copy-start(u32[32]{0:T(128)} %constant.51) | copy-start | bytes 388
  40.6 31.0 %copy-start.6 = (s32[64,2]{0,1:T(2,128)S(1)}, s32[64,2]{0,1:T(2,128)}, u32[]{:S(2)}) copy-start(s32[64,2]{0,1:T(2,128)} %param.33) | copy-start | bytes 1540
  87.9 63.1 %reduce-scatter.2.cloned.1.call-start = ((), (), s32[]{:S(2)}) async-start(), calls=%async_computation.4 | async-start | bytes 1310720 | tf_op jit(solution)/shard_map/reduce_scatter | solution.py:128
  115.5 49.8 %copy-start.7 = (f32[64,2]{0,1:T(2,128)S(1)}, f32[64,2]{0,1:T(2,128)}, u32[]{:S(2)}) copy-start(f32[64,2]{0,1:T(2,128)} %param.34) | copy-start | bytes 1540
  151.0 14.3 %all-to-all-start.1 = ((bf16[8,32,512]{2,1,0:T(8,128)(2,1)}), bf16[8,32,512]{2,1,0:T(8,128)(2,1)S(1)}, u32[]{:S(2)}, u32[]{:S(2)}) async-start(bf16[8,32,512]{2,1,0:T(8,128)(2,1)} %bitcast.97), calls=%async_computation.2 | async-start | bytes 524288 | tf_op jit(solution)/shard_map/all_to_all | solution.py:134
Sparse Core Ops, SparseCore 0:
  88.0 23.6 all-gather.2
  123.0 27.9 reduce-scatter.1
